TPU v7x, 32 devices: a whole 2x2x4 slice. The times are simulated.
32 devices in a mesh: sp: 8 (over z, core), tp: 4 (over y, x).
Axes of the slice: x: 2, y: 2, z: 4, core: 2. Of those that a mesh axis runs over, the one named last changes fastest.
Arguments:
- routes: int32 [1536, 2], P('sp'), may hold values from 0 to 7, all different within a row; in each aligned block of 192 rows (0 to 191, 192 to 383, ...) at most 72 rows name the same one
- route_weights: float32 [1536, 2], P('sp'), may hold values from 0.2 to 1
- expert_inputs: bfloat16 [1536, 2048], P('sp', 'tp'), may hold values from -6 to 6
- out_grad: bfloat16 [1536, 2048], P('sp', 'tp'), may hold values from -6 to 6
- w_gate: bfloat16 [8, 2816, 2048], P('sp', 'tp'), may hold values from -0.125 to 0.125
- w_up: bfloat16 [8, 2816, 2048], P('sp', 'tp'), may hold values from -0.125 to 0.125
- w_down: bfloat16 [8, 2816, 2048], P('sp', 'tp'), may hold values from -0.109375 to 0.109375
- conv_u: bfloat16 [1536, 512], P('sp', 'tp'), may hold values from -6 to 6
- conv_b: bfloat16 [1536, 512], P('sp', 'tp'), may hold values from -6 to 6
- conv_c: bfloat16 [1536, 512], P('sp', 'tp'), may hold values from -6 to 6
- conv_taps: float32 [3, 512], P(None, 'tp'), may hold values from -3 to 3
- out_proj: bfloat16 [512, 2048], P('tp'), may hold values from -0.25 to 0.25
Outputs:
- grad_w_gate: bfloat16 [8, 2816, 2048], P('sp', 'tp')
- grad_w_up: bfloat16 [8, 2816, 2048], P('sp', 'tp')
- grad_w_down: bfloat16 [8, 2816, 2048], P('sp', 'tp')
- grad_input: bfloat16 [1536, 2048], P('sp', 'tp')
- grad_proj: float32 [2048, 512], P('sp', 'tp')
- grad_u: bfloat16 [1536, 512], P('sp', 'tp')
- grad_b: bfloat16 [1536, 512], P('sp', 'tp')
- grad_c: bfloat16 [1536, 512], P('sp', 'tp')
Inputs may be any that keep to these rules, and one draw needn't show every extreme that they name: `routes`: each row names two different experts. In each aligned block of 192 rows no expert is named more than 72 times, a bound that some block reaches.
All inputs are finite; a program needn't handle non-finite values.
Results may differ from a plain program's by a relative error of at most 0.025.
Values may be sent and summed in bfloat16 or wider, within the bound.
A program may use at most 64 MiB of HBM per device.

v0:
```python
import jax
import jax.numpy as jnp
from jax import lax
from jax.sharding import PartitionSpec as P


def extended(value, sides, width):
    for axis, dim in sides:
        size, length = (lax.axis_size(axis), value.shape[dim])
        up = [(i, (i + 1) % size) for i in range(size - 1)]
        down = [(j, i) for i, j in up]
        last = lax.slice_in_dim(value, length - width, length, axis=dim)
        leading = lax.slice_in_dim(value, 0, width, axis=dim)
        before = lax.ppermute(last, axis, up)
        after = lax.ppermute(leading, axis, down)
        value = jnp.concatenate([before, value, after], axis=dim)
    return value


def contract_first(left, right):
    return lax.dot_general(
        left, right, (((0,), (0,)), ((), ())), preferred_element_type=jnp.float32
    )


def contract_last(left, right):
    return lax.dot_general(
        left, right, (((1,), (1,)), ((), ())), preferred_element_type=jnp.float32
    )


def slot_tables(routes, capacity, experts):
    flat_expert = routes.reshape(-1)
    columns = lax.broadcasted_iota(jnp.int32, (flat_expert.shape[0], experts), 1)
    onehot = (flat_expert[:, None] == columns).astype(jnp.int32)
    before = jnp.cumsum(onehot, axis=0) - onehot
    slot_rank = jnp.sum(before * onehot, axis=1)
    slot_index = flat_expert * capacity + slot_rank
    labels = jnp.arange(flat_expert.shape[0], dtype=jnp.int32) + 1
    slot_owner = jnp.zeros((experts * capacity,), jnp.int32).at[slot_index].set(labels)
    return (slot_index, slot_owner)


def expert_backward(rows, grads, gate_weight, up_weight, down_weight):
    gate_pre = contract_last(rows, gate_weight)
    up_pre = contract_last(rows, up_weight)
    gate_act = jax.nn.silu(gate_pre)
    hidden = (gate_act * up_pre).astype(jnp.bfloat16)
    grad_down = contract_first(hidden, grads).astype(jnp.bfloat16)
    grad_hidden = contract_last(grads, down_weight)
    sigma = jax.nn.sigmoid(gate_pre)
    gate_back = (grad_hidden * up_pre * sigma * (1.0 + gate_pre * (1.0 - sigma))).astype(
        jnp.bfloat16
    )
    up_back = (grad_hidden * gate_act).astype(jnp.bfloat16)
    grad_gate = contract_first(gate_back, rows).astype(jnp.bfloat16)
    grad_up = contract_first(up_back, rows).astype(jnp.bfloat16)
    return (grad_gate, grad_up, grad_down, gate_back, up_back)


def body(
    routes,
    route_weights,
    expert_inputs,
    out_grad,
    w_gate,
    w_up,
    w_down,
    conv_u,
    conv_b,
    conv_c,
    conv_taps,
    out_proj,
):
    f32 = jnp.float32
    bf16 = jnp.bfloat16
    experts = lax.axis_size("sp")
    tok_local = routes.shape[0]
    capacity = 3 * tok_local // experts
    slot_index, slot_owner = slot_tables(routes, capacity, experts)
    filled = (slot_owner > 0)[:, None]
    picked = jnp.maximum(slot_owner - 1, 0)
    repeated = jnp.repeat(expert_inputs, 2, axis=0)
    scaled = (route_weights[:, :, None] * out_grad.astype(f32)[:, None, :]).astype(bf16)
    scaled = scaled.reshape(2 * tok_local, out_grad.shape[1])
    send_rows = jnp.where(filled, repeated[picked], jnp.zeros((), bf16))
    send_grads = jnp.where(filled, scaled[picked], jnp.zeros((), bf16))
    send_rows, send_grads = (send_rows, send_grads)
    part_rows, part_grads = (
        lax.all_to_all(send_rows, "sp", split_axis=0, concat_axis=0, tiled=True),
        lax.all_to_all(send_grads, "sp", split_axis=0, concat_axis=0, tiled=True),
    )
    rows, grads = (
        lax.all_gather(part_rows, "tp", axis=1, tiled=True),
        lax.all_gather(part_grads, "tp", axis=1, tiled=True),
    )
    gate_weight = w_gate[0]
    up_weight = w_up[0]
    grad_gate, grad_up, grad_down, gate_back, up_back = expert_backward(
        rows, grads, gate_weight, up_weight, w_down[0]
    )
    partial_value = jnp.dot(gate_back, gate_weight, preferred_element_type=f32) + jnp.dot(
        up_back, up_weight, preferred_element_type=f32
    )
    summed = (
        lax.psum_scatter(partial_value.astype(bf16), "tp", scatter_dimension=1, tiled=True)
        .astype(jnp.float32)
        .astype(bf16)
    )
    returned = lax.all_to_all(summed, "sp", split_axis=0, concat_axis=0, tiled=True)
    picked_back = returned[slot_index].astype(f32).reshape(tok_local, 2, returned.shape[1])
    grad_input = (out_grad.astype(f32) + picked_back[:, 0] + picked_back[:, 1]).astype(bf16)
    mixed_in = conv_c.astype(f32) * conv_u.astype(f32)
    padded = extended(mixed_in, (("sp", 0),), 1)
    convolved = (
        conv_taps[0] * padded[0:tok_local]
        + conv_taps[1] * padded[1 : tok_local + 1]
        + conv_taps[2] * padded[2 : tok_local + 2]
    )
    conv_out = (conv_b.astype(f32) * convolved).astype(bf16)
    grad_full = lax.all_gather(grad_input, "tp", axis=1, tiled=True)
    grad_conv = contract_last(grad_full, out_proj)
    grad_b = (grad_conv * convolved).astype(bf16)
    grad_mixed = grad_conv * conv_b.astype(f32)
    rim = extended(grad_mixed, (("sp", 0),), 1)
    grad_z = (
        conv_taps[0] * rim[2 : tok_local + 2]
        + conv_taps[1] * rim[1 : tok_local + 1]
        + conv_taps[2] * rim[0:tok_local]
    )
    grad_c = (grad_z * conv_u.astype(f32)).astype(bf16)
    grad_u = (grad_z * conv_c.astype(f32)).astype(bf16)
    grad_proj = lax.psum_scatter(
        contract_first(grad_full, conv_out).astype(jnp.bfloat16),
        "sp",
        scatter_dimension=0,
        tiled=True,
    ).astype(jnp.float32)
    return (
        grad_gate[None],
        grad_up[None],
        grad_down[None],
        grad_input,
        grad_proj,
        grad_u,
        grad_b,
        grad_c,
    )


def solution(mesh):
    in_specs = (
        P("sp", None),
        P("sp", None),
        P("sp", "tp"),
        P("sp", "tp"),
        P("sp", "tp", None),
        P("sp", "tp", None),
        P("sp", "tp", None),
        P("sp", "tp"),
        P("sp", "tp"),
        P("sp", "tp"),
        P(None, "tp"),
        P("tp", None),
    )
    out_specs = (
        P("sp", "tp", None),
        P("sp", "tp", None),
        P("sp", "tp", None),
        P("sp", "tp"),
        P("sp", "tp"),
        P("sp", "tp"),
        P("sp", "tp"),
        P("sp", "tp"),
    )
    return jax.shard_map(body, mesh=mesh, in_specs=in_specs, out_specs=out_specs, check_vma=False)
```

profile of v0, /device:TPU:0, one launch (start us, length us, event | category | flops | bytes accessed | tf_op | source)
XLA Modules:
  0.0 277.0 jit_solution(8447588597194261662)
XLA Ops:
  7.2 0.8 broadcast_multiply_fusion
  8.1 0.9 copy.23
  9.0 0.1 eq.21
  9.4 0.1 mul.127
  9.5 0.9 reduce-window.6
  10.4 0.2 slice_reduce_fusion
  10.8 2.9 %scatter_custom_fusion = s32[576]{0:T(1024)S(1)} fusion(s32[384]{0:T(512)S(1)} %fusion.35, s32[384]{0:T(512)S(1)} %iota_add_fusion, s32[]{:T(128)} %constant.7.clone.1), kind=kCustom, calls=%fused_computation.68 | custom fusion | bytes 2308 | tf_op jit(solution)/shard_map/scatter | solution.py:40
  13.7 2.0 mul.131
  15.8 2.6 mul.132
  18.4 0.1 mul.129
  18.7 1.0 broadcast_in_dim.43
  19.6 1.1 reshape.92
  20.8 2.0 multiply_convert_fusion.4
  22.8 4.3 %gather_fusion = bf16[576,512]{1,0:T(8,128)(2,1)} fusion(bf16[384,512]{1,0:T(8,128)(2,1)} %multiply_convert_fusion.4, s32[1024]{0:T(1024)S(1)} %pad_clamp_fusion.1), kind=kCustom, calls=%fused_computation | custom fusion | bytes 1181952 | tf_op jit(solution)/shard_map/gather | solution.py:87
  27.1 3.2 %gather_fusion.1 = bf16[576,512]{1,0:T(8,128)(2,1)} fusion(bf16[384,512]{1,0:T(8,128)(2,1)S(1)} %reshape.92, s32[1024]{0:T(1024)S(1)} %pad_clamp_fusion.1), kind=kCustom, calls=%fused_computation.1 | custom fusion | bytes 1181952 | tf_op jit(solution)/shard_map/gather | solution.py:86
  30.4 1.4 broadcast_select_fusion.1
  31.8 23.0 %all_to_all.30 = bf16[8,72,512]{2,1,0:T(8,128)(2,1)} all-to-all(bf16[8,72,512]{2,1,0:T(8,128)(2,1)S(1)} %get-tuple-element.23), channel_id=1, replica_groups=mesh['sp'=8,'tp'=4] {'sp'}, dimensions={0} | all-to-all | bytes 1179648 | tf_op jit(solution)/shard_map/all_to_all | solution.py:90
  54.8 19.8 %all_to_all.31 = bf16[8,72,512]{2,1,0:T(8,128)(2,1)} all-to-all(bf16[8,72,512]{2,1,0:T(8,128)(2,1)S(1)} %get-tuple-element.22), channel_id=1, replica_groups=mesh['sp'=8,'tp'=4] {'sp'}, dimensions={0} | all-to-all | bytes 1179648 | tf_op jit(solution)/shard_map/all_to_all | solution.py:91
  74.7 0.2 reduce-scatter.3.cloned.1.call-start
  74.9 16.2 %all-gather.5.cloned.1.call-done = bf16[576,2048]{1,0:T(8,128)(2,1)} async-done(((bf16[576,512]{1,0:T(8,128)(2,1)}), bf16[576,2048]{1,0:T(8,128)(2,1)}) %all-gather.5.cloned.1.call-update) | async-done | bytes 2359312 | tf_op jit(solution)/shard_map/all_gather | solution.py:94
  91.1 5.1 %fusion.5 = f32[576,704]{1,0:T(8,128)} fusion(bf16[576,2048]{1,0:T(8,128)(2,1)} %all-gather.5.cloned.1.call-done, bf16[1,704,2048]{2,1,0:T(8,128)(2,1)S(1)} %copy-done), kind=kOutput, calls=%fused_computation.13 | convolution fusion | flops 1660944384 | bytes 6864896 | tf_op jit(solution)/shard_map/dot_general | solution.py:27
  96.2 3.3 %fusion.8 = f32[576,704]{1,0:T(8,128)} fusion(bf16[576,2048]{1,0:T(8,128)(2,1)S(1)} %copy-done.12, bf16[1,704,2048]{2,1,0:T(8,128)(2,1)S(1)} %copy-done.10), kind=kOutput, calls=%fused_computation.16 | convolution fusion | flops 1660944384 | bytes 6864896 | tf_op jit(solution)/shard_map/dot_general | solution.py:27
  99.5 30.7 %all-gather.3.cloned.1.call-done = bf16[576,2048]{1,0:T(8,128)(2,1)} async-done(((bf16[576,512]{1,0:T(8,128)(2,1)}), bf16[576,2048]{1,0:T(8,128)(2,1)}) %all-gather.3.cloned.1.call-update) | async-done | bytes 2359312 | tf_op jit(solution)/shard_map/all_gather | solution.py:95
  130.2 6.0 %multiply_convert_fusion.1 = (bf16[576,704]{1,0:T(8,128)(2,1)S(1)}, bf16[576,704]{1,0:T(8,128)(2,1)S(1)}) fusion(f32[576,704]{1,0:T(8,128)} %fusion.5, f32[576,704]{1,0:T(8,128)} %fusion.8, bf16[576,2048]{1,0:T(8,128)(2,1)} %all-gather.3.cloned.1.call-done, bf16[1,704,2048]{2,1,0:T(8,128)(2,1)} %param.18), kind=kOutput, calls=%fused_computation.22 | convolution fusion | flops 1666215936 | bytes 10108928 | tf_op jit(solution)/shard_map/dot_general | solution.py:27
  136.2 2.0 fusion.3
  138.2 0.4 copy-done.11
  138.7 3.4 %add_convert_fusion = bf16[576,2048]{1,0:T(8,128)(2,1)} fusion(f32[576,2048]{1,0:T(8,128)S(1)} %fusion.3, bf16[576,704]{1,0:T(8,128)(2,1)S(1)} %get-tuple-element.8, bf16[1,704,2048]{2,1,0:T(8,128)(2,1)S(1)} %copy-done.11), kind=kOutput, calls=%fused_computation.4 | convolution fusion | flops 1663303680 | bytes 10772480 | tf_op jit(solution)/shard_map/dot_general | solution.py:102
  142.1 37.5 %reduce-scatter.3.cloned.1.call-done = bf16[576,512]{1,0:T(8,128)(2,1)} async-done(((bf16[576,2048]{1,0:T(8,128)(2,1)}), bf16[576,512]{1,0:T(8,128)(2,1)}) %reduce-scatter.3.cloned.1.call-update) | async-done | bytes 589840 | tf_op jit(solution)/shard_map/reduce_scatter | solution.py:106
  179.6 4.6 %all-to-all-start.2 = ((bf16[8,72,512]{2,1,0:T(8,128)(2,1)}), bf16[8,72,512]{2,1,0:T(8,128)(2,1)S(1)}, u32[]{:S(2)}, u32[]{:S(2)}) async-start(bf16[8,72,512]{2,1,0:T(8,128)(2,1)} %bitcast.72), calls=%async_computation.3 | async-start | bytes 1179648 | tf_op jit(solution)/shard_map/all_to_all | solution.py:110
  184.3 16.7 %all-to-all-done.2 = bf16[8,72,512]{2,1,0:T(8,128)(2,1)S(1)} async-done(((bf16[8,72,512]{2,1,0:T(8,128)(2,1)}), bf16[8,72,512]{2,1,0:T(8,128)(2,1)S(1)}, u32[]{:S(2)}, u32[]{:S(2)}) %all-to-all-start.2) | async-done | bytes 589856 | tf_op jit(solution)/shard_map/all_to_all | solution.py:110
  200.9 2.6 gather_fusion.2
  203.5 2.4 reshape.93
  205.9 2.1 fusion.38
  208.2 11.6 %all_gather.11 = bf16[192,2048]{1,0:T(8,128)(2,1)S(1)} all-gather(bf16[192,512]{1,0:T(8,128)(2,1)S(1)} %fusion.14), channel_id=1, replica_groups=mesh['sp'=8,'tp'=4] {'tp'}, dimensions={1}, use_global_device_ids=true | all-gather | bytes 983040 | tf_op jit(solution)/shard_map/all_gather | solution.py:121
  219.8 0.4 convert_multiply_fusion.3
  220.2 1.3 collective-permute-start.3
  221.5 1.3 collective-permute-start.2
  222.8 1.7 collective-permute-done.2
  224.5 0.7 fusion.19
  225.2 1.3 collective-permute-start.1
  226.5 4.4 %collective-permute-start = (f32[1,128]{1,0:T(1,128)S(1)}, f32[1,128]{1,0:T(1,128)S(1)}, u32[]{:S(2)}, u32[]{:S(2)}) collective-permute-start(f32[1,128]{1,0:T(1,128)S(1)} %get-tuple-element.17), channel_id=1, source_target_pairs={{0,4},{4,8},{8,12},{12,16},{16,20},{20,24},{24,28},{1,5},{5,9},{9,... | collective-permute-start | bytes 1544 | tf_op jit(solution)/shard_map/ppermute | solution.py:14
  231.0 4.0 %fusion = bf16[1,704,2048]{2,1,0:T(8,128)(2,1)} fusion(bf16[576,704]{1,0:T(8,128)(2,1)S(1)} %copy-done.16, bf16[576,2048]{1,0:T(8,128)(2,1)S(1)} %copy-done.13), kind=kOutput, calls=%fused_computation.8 | convolution fusion | flops 1662386176 | bytes 6053888 | tf_op jit(solution)/shard_map/dot_general | solution.py:21
  235.0 1.3 convolution_convert_fusion.3
  236.4 6.1 %fusion.1 = bf16[1,704,2048]{2,1,0:T(8,128)(2,1)} fusion(bf16[576,704]{1,0:T(8,128)(2,1)} %copy-done.17, bf16[576,2048]{1,0:T(8,128)(2,1)} %all-gather.5.cloned.1.call-done), kind=kOutput, calls=%fused_computation.9 | convolution fusion | flops 1662386176 | bytes 6053888 | tf_op jit(solution)/shard_map/dot_general | solution.py:21
  242.5 4.1 %fusion.2 = bf16[1,704,2048]{2,1,0:T(8,128)(2,1)} fusion(bf16[576,2048]{1,0:T(8,128)(2,1)S(1)} %copy-done.14, f32[576,704]{1,0:T(8,128)S(1)} %copy-done.19, f32[576,704]{1,0:T(8,128)S(1)} %copy-done.18), kind=kOutput, calls=%fused_computation.10 | convolution fusion | flops 1664819200 | bytes 8486912 | tf_op jit(solution)/shard_map/dot_general | solution.py:21
  246.6 0.7 multiply_convert_fusion.5
  247.2 21.7 %reduce-scatter.5.cloned.1.call-done = bf16[256,128]{1,0:T(8,128)(2,1)} async-done(((bf16[2048,128]{1,0:T(8,128)(2,1)}), bf16[256,128]{1,0:T(8,128)(2,1)}) %reduce-scatter.5.cloned.1.call-update) | async-done | bytes 65552 | tf_op jit(solution)/shard_map/reduce_scatter | solution.py:133
  269.0 1.5 convert_element_type.97
  (66 shorter events, 1.0 us)
Async XLA Ops:
  7.2 83.9 %copy-start = (bf16[1,704,2048]{2,1,0:T(8,128)(2,1)S(1)}, bf16[1,704,2048]{2,1,0:T(8,128)(2,1)}, u32[]{:S(2)}) copy-start(bf16[1,704,2048]{2,1,0:T(8,128)(2,1)} %param.16) | copy-start | bytes 8650756
  7.2 11.1 %copy-start.8 = (f32[192,2]{0,1:T(2,128)S(1)}, f32[192,2]{0,1:T(2,128)}, u32[]{:S(2)}) copy-start(f32[192,2]{0,1:T(2,128)} %param.13) | copy-start | bytes 4612
  7.2 11.5 %copy-start.5 = (bf16[192,512]{1,0:T(8,128)(2,1)S(1)}, bf16[192,512]{1,0:T(8,128)(2,1)}, u32[]{:S(2)}) copy-start(bf16[192,512]{1,0:T(8,128)(2,1)} %param.14) | copy-start | bytes 589828
  7.2 83.9 %all-gather.5.cloned.1.call-start = ((), (), s32[]{:S(2)}) async-start(), calls=%async_computation.6 | async-start | bytes 2949120 | tf_op jit(solution)/shard_map/all_gather | solution.py:94
  54.8 75.4 %all-gather.3.cloned.1.call-start = ((), (), s32[]{:S(2)}) async-start(), calls=%async_computation.5 | async-start | bytes 2949120 | tf_op jit(solution)/shard_map/all_gather | solution.py:95
  74.7 104.9 %reduce-scatter.3.cloned.1.call-start = ((), (), s32[]{:S(2)}) async-start(), calls=%async_computation.7 | async-start | bytes 2949120 | tf_op jit(solution)/shard_map/reduce_scatter | solution.py:106
  91.1 5.1 %copy-start.10 = (bf16[1,704,2048]{2,1,0:T(8,128)(2,1)S(1)}, bf16[1,704,2048]{2,1,0:T(8,128)(2,1)}, u32[]{:S(2)}) copy-start(bf16[1,704,2048]{2,1,0:T(8,128)(2,1)} %param.17) | copy-start | bytes 8650756
  91.1 5.1 %copy-start.12 = (bf16[576,2048]{1,0:T(8,128)(2,1)S(1)}, bf16[576,2048]{1,0:T(8,128)(2,1)}, u32[]{:S(2)}) copy-start(bf16[576,2048]{1,0:T(8,128)(2,1)} %all-gather.5.cloned.1.call-done) | copy-start | bytes 7077892
  136.2 2.0 copy-start.15
  136.2 2.0 copy-start.17
  136.2 2.5 copy-start.11
  179.6 21.3 %all-to-all-start.2 = ((bf16[8,72,512]{2,1,0:T(8,128)(2,1)}), bf16[8,72,512]{2,1,0:T(8,128)(2,1)S(1)}, u32[]{:S(2)}, u32[]{:S(2)}) async-start(bf16[8,72,512]{2,1,0:T(8,128)(2,1)} %bitcast.72), calls=%async_computation.3 | async-start | bytes 1179648 | tf_op jit(solution)/shard_map/all_to_all | solution.py:110
  184.2 84.8 %reduce-scatter.5.cloned.1.call-start = ((), (), s32[]{:S(2)}) async-start(), calls=%async_computation.8 | async-start | bytes 589824 | tf_op jit(solution)/shard_map/reduce_scatter | solution.py:133
  203.5 4.6 %copy-start.1 = (bf16[192,512]{1,0:T(8,128)(2,1)S(1)}, bf16[192,512]{1,0:T(8,128)(2,1)}, u32[]{:S(2)}) copy-start(bf16[192,512]{1,0:T(8,128)(2,1)} %param.15) | copy-start | bytes 589828
  203.5 16.2 %copy-start.4 = (bf16[192,128]{1,0:T(8,128)(2,1)S(1)}, bf16[192,128]{1,0:T(8,128)(2,1)}, u32[]{:S(2)}) copy-start(bf16[192,128]{1,0:T(8,128)(2,1)} %param.20) | copy-start | bytes 147460
  205.9 13.8 %copy-start.3 = (bf16[128,2048]{1,0:T(8,128)(2,1)S(1)}, bf16[128,2048]{1,0:T(8,128)(2,1)}, u32[]{:S(2)}) copy-start(bf16[128,2048]{1,0:T(8,128)(2,1)} %param.23) | copy-start | bytes 1572868
  205.9 16.8 %copy-start.9 = (f32[3,128]{1,0:T(4,128)S(1)}, f32[3,128]{1,0:T(4,128)}, u32[]{:S(2)}) copy-start(f32[3,128]{1,0:T(4,128)} %param.22) | copy-start | bytes 4612
  205.9 18.6 %copy-start.6 = (bf16[192,128]{1,0:T(8,128)(2,1)S(1)}, bf16[192,128]{1,0:T(8,128)(2,1)}, u32[]{:S(2)}) copy-start(bf16[192,128]{1,0:T(8,128)(2,1)} %param.19) | copy-start | bytes 147460
  205.9 18.6 %copy-start.7 = (bf16[192,128]{1,0:T(8,128)(2,1)S(1)}, bf16[192,128]{1,0:T(8,128)(2,1)}, u32[]{:S(2)}) copy-start(bf16[192,128]{1,0:T(8,128)(2,1)} %param.21) | copy-start | bytes 147460
  208.0 22.9 %copy-start.13 = (bf16[576,2048]{1,0:T(8,128)(2,1)S(1)}, bf16[576,2048]{1,0:T(8,128)(2,1)}, u32[]{:S(2)}) copy-start(bf16[576,2048]{1,0:T(8,128)(2,1)} %all-gather.5.cloned.1.call-done) | copy-start | bytes 7077892
  208.1 22.9 %copy-start.16 = (bf16[576,704]{1,0:T(8,128)(2,1)S(1)}, bf16[576,704]{1,0:T(8,128)(2,1)}, u32[]{:S(2)}) copy-start(bf16[576,704]{1,0:T(8,128)(2,1)} %copy-done.15) | copy-start | bytes 2433028
  208.2 26.8 %copy-start.2 = (bf16[192,512]{1,0:T(8,128)(2,1)}, bf16[192,512]{1,0:T(8,128)(2,1)S(1)}, u32[]{:S(2)}) copy-start(bf16[192,512]{1,0:T(8,128)(2,1)S(1)} %fusion.14) | copy-start | bytes 589828
  220.2 2.6 collective-permute-start.3
  221.5 3.1 %collective-permute-start.2 = (f32[1,128]{1,0:T(1,128)S(1)}, f32[1,128]{1,0:T(1,128)S(1)}, u32[]{:S(2)}, u32[]{:S(2)}) collective-permute-start(f32[1,128]{1,0:T(1,128)S(1)} %get-tuple-element.15), channel_id=1, source_target_pairs={{4,0},{8,4},{12,8},{16,12},{20,16},{24,20},{28,24},{5,1},{9,5},{13... | collective-permute-start | bytes 1544 | tf_op jit(solution)/shard_map/ppermute | solution.py:15
  225.2 9.8 %collective-permute-start.1 = (f32[1,128]{1,0:T(1,128)S(1)}, f32[1,128]{1,0:T(1,128)S(1)}, u32[]{:S(2)}, u32[]{:S(2)}) collective-permute-start(f32[1,128]{1,0:T(1,128)S(1)} %get-tuple-element.18), channel_id=1, source_target_pairs={{4,0},{8,4},{12,8},{16,12},{20,16},{24,20},{28,24},{5,1},{9,5},{13... | collective-permute-start | bytes 1544 | tf_op jit(solution)/shard_map/ppermute | solution.py:15
  226.5 8.5 %collective-permute-start = (f32[1,128]{1,0:T(1,128)S(1)}, f32[1,128]{1,0:T(1,128)S(1)}, u32[]{:S(2)}, u32[]{:S(2)}) collective-permute-start(f32[1,128]{1,0:T(1,128)S(1)} %get-tuple-element.17), channel_id=1, source_target_pairs={{0,4},{4,8},{8,12},{12,16},{16,20},{20,24},{24,28},{1,5},{5,9},{9,... | collective-permute-start | bytes 1544 | tf_op jit(solution)/shard_map/ppermute | solution.py:14
  236.3 6.1 %copy-start.14 = (bf16[576,2048]{1,0:T(8,128)(2,1)S(1)}, bf16[576,2048]{1,0:T(8,128)(2,1)}, u32[]{:S(2)}) copy-start(bf16[576,2048]{1,0:T(8,128)(2,1)} %all-gather.3.cloned.1.call-done) | copy-start | bytes 7077892
  236.4 6.1 %copy-start.18 = (f32[576,704]{1,0:T(8,128)S(1)}, f32[576,704]{1,0:T(8,128)}, u32[]{:S(2)}) copy-start(f32[576,704]{1,0:T(8,128)} %fusion.5) | copy-start | bytes 4866052
  236.4 6.1 %copy-start.19 = (f32[576,704]{1,0:T(8,128)S(1)}, f32[576,704]{1,0:T(8,128)}, u32[]{:S(2)}) copy-start(f32[576,704]{1,0:T(8,128)} %fusion.8) | copy-start | bytes 4866052
Sparse Core Ops, SparseCore 0:
  54.9 36.1 all-gather.4
  92.9 37.1 all-gather.2
  142.2 37.3 reduce-scatter.2
  236.5 32.4 reduce-scatter.4
where the time goes:
time: 278 us; the launch traced here: 277 us
  waiting for transfers between devices  125 us (45%)
  blocking collectives  54.4 us (20%)
  matrix products  35.7 us (13%)
  local copies, waits for them, and re-layouts  26.8 us (10%)
  between operations  14.1 us (5%)
  starting transfers between devices  13.2 us (5%)
  other arithmetic  8.24 us (3%)
    reduce_scatter x1, waiting for transfers between devices, body(): lax.psum_scatter(partial_value.astype(bf16), 'tp', scatter_dimension=1, t...  37.5 us
    all_gather x1, waiting for transfers between devices, body(): lax.all_gather(part_grads, 'tp', axis=1, tiled=True)  30.7 us
    all_to_all x1, blocking collectives, body(): lax.all_to_all(send_rows, 'sp', split_axis=0, concat_axis=0, tiled=True)  23 us
    reduce_scatter x1, waiting for transfers between devices, body(): lax.psum_scatter(contract_first(grad_full, conv_out).astype(jnp.bfloat16)...  21.7 us
    all_to_all x1, blocking collectives, body(): lax.all_to_all(send_grads, 'sp', split_axis=0, concat_axis=0, tiled=True)  19.8 us
    all_to_all x1, waiting for transfers between devices, body(): lax.all_to_all(summed, 'sp', split_axis=0, concat_axis=0, tiled=True)  16.7 us
    all_gather x1, waiting for transfers between devices, body(): lax.all_gather(part_rows, 'tp', axis=1, tiled=True)  16.2 us
    dot_general x4, matrix products, contract_first(): lax.dot_general(left, right, (((0,), (0,)), ((), ())), preferred_element_...  15.5 us
  transfers between devices with their start and end apart: 9, of which 6 were waited for; matrix products, arithmetic and copies ran while one was open for 8% of the time, Pallas kernels for 0%

commit v1 on v0

v1 whole, which is shorter than its diff:
```python
import functools

import jax
import jax.numpy as jnp
from jax import lax
from jax.experimental import pallas as pl
from jax.experimental.pallas import tpu as pltpu
from jax.sharding import PartitionSpec as P

MESH = pl.DeviceIdType.MESH
F32 = jnp.float32
BF16 = jnp.bfloat16


def contract_first(left, right):
    return lax.dot_general(
        left, right, (((0,), (0,)), ((), ())), preferred_element_type=jnp.float32
    )


def contract_last(left, right):
    return lax.dot_general(
        left, right, (((1,), (1,)), ((), ())), preferred_element_type=jnp.float32
    )


def loop(count, step):
    lax.fori_loop(0, count, lambda i, c: (step(i), c)[1], 0)


def enter(sizes):
    barrier = pltpu.get_barrier_semaphore()
    for axis, size in sizes:
        me = lax.axis_index(axis)

        def greet(i, axis=axis, size=size, me=me):
            pl.semaphore_signal(
                barrier,
                inc=1,
                device_id={axis: lax.rem(me + i + 1, size)},
                device_id_type=MESH,
            )

        loop(size - 1, greet)
    return lambda: pl.semaphore_wait(barrier, sum(size - 1 for _, size in sizes))


def remote(src, dst, send, recv, **where):
    return pltpu.make_async_remote_copy(
        src_ref=src,
        dst_ref=dst,
        send_sem=send,
        recv_sem=recv,
        device_id=where,
        device_id_type=MESH,
    )


def members(routes, experts):
    count = routes.shape[0]
    columns = lax.broadcasted_iota(jnp.int32, (count, experts), 1)
    first = (routes[:, 0:1] == columns).astype(F32)
    second = (routes[:, 1:2] == columns).astype(F32)
    return first, second


def triangle(count, earlier_dim):
    a = lax.broadcasted_iota(jnp.int32, (count, count), earlier_dim)
    b = lax.broadcasted_iota(jnp.int32, (count, count), 1 - earlier_dim)
    return (a < b).astype(F32).astype(BF16), (a == b).astype(F32).astype(BF16)


def dispatch_kernel(
    S, T, routes_ref, wts_ref, xin_ref, gin_ref, x_ref, g_ref,
    xs, gs, zsend, zrecv, fsend, frecv, rsend, rrecv, lsem,
):
    s, p = lax.axis_index("sp"), lax.axis_index("tp")
    cap, d = xs.shape[1], xs.shape[2]
    wait_entry = enter((("sp", S), ("tp", T)))

    routes = routes_ref[...]
    first, second = members(routes, S)
    weight = first * wts_ref[:, 0:1] + second * wts_ref[:, 1:2]
    member = (first + second).astype(BF16)
    tri, eye = triangle(routes.shape[0], 0)
    rank = contract_first(member, tri)
    named = contract_first(member, eye)
    code = jnp.where(named > 0.5, rank, -1.0).astype(jnp.int32)
    slots = lax.broadcasted_iota(jnp.int32, (cap, routes.shape[0]), 0)
    xin = xin_ref[...]
    gin = gin_ref[...].astype(F32)
    for e in range(S):
        pick = (slots == code[e : e + 1, :]).astype(F32).astype(BF16)
        xs[e] = jnp.dot(pick, xin, preferred_element_type=F32).astype(BF16)
        scaled = (weight[:, e : e + 1] * gin).astype(BF16)
        gs[e] = jnp.dot(pick, scaled, preferred_element_type=F32).astype(BF16)
    wait_entry()

    arrays = ((xs, x_ref), (gs, g_ref))

    def cols(q, half=None):
        if half is None:
            return pl.ds(pl.multiple_of(q * d, d), d)
        return pl.ds(pl.multiple_of(q * d + half * (d // 2), d // 2), d // 2)

    def origin(o):
        return lax.rem(s - o + S, S)

    def zcopy(i, o, arriving=False):
        src, out = arrays[i]
        dst = lax.rem(s + o, S)
        row = origin(o) if arriving else s
        return remote(
            src.at[dst], out.at[row, :, cols(p)], zsend.at[i, o], zrecv.at[i, o], sp=dst
        )

    locals_ = [
        pltpu.make_async_copy(src.at[s], out.at[s, :, cols(p)], lsem.at[i])
        for i, (src, out) in enumerate(arrays)
    ]
    for i in range(2):
        locals_[i].start()
        loop(S - 1, lambda k, i=i: zcopy(i, k + 1).start())

    relay = T == 4
    if relay:
        xn, yn = p + 1 - 2 * lax.rem(p, 2), lax.rem(p + 2, 4)
        partners = ((xn, xn), (yn, yn))
    else:
        partners = tuple(
            (lax.rem(p + r, T), lax.rem(p - r + T, T)) for r in range(1, T)
        )

    def fcopy(i, o, k, arriving=False):
        out = arrays[i][1]
        to, whence = partners[k]
        view = out.at[origin(o), :, cols(whence if arriving else p)]
        return remote(view, view, fsend.at[i, o, k], frecv.at[i, o, k], tp=to)

    def rcopy(i, o, k, arriving=False):
        out = arrays[i][1]
        near, far = ((xn, yn), (yn, xn))[k]
        view = out.at[origin(o), :, cols(3 - p if arriving else near, k)]
        return remote(view, view, rsend.at[i, o, k], rrecv.at[i, o, k], tp=far)

    def forward(i, o):
        @pl.when(o > 0)
        def _():
            zcopy(i, o, True).wait_recv()

        for k in range(len(partners)):
            fcopy(i, o, k).start()

    def pass_on(i, o):
        for k in range(len(partners)):
            fcopy(i, o, k, True).wait_recv()
            if relay:
                rcopy(i, o, k).start()

    for i in range(2):
        locals_[i].wait()
        forward(i, 0)
        if i == 1:
            pass_on(0, S - 1)

        def step(k, i=i):
            forward(i, k + 1)
            pass_on(i, k)

        loop(S - 1, step)
    pass_on(1, S - 1)
    for i in range(2):
        loop(S - 1, lambda k, i=i: zcopy(i, k + 1).wait_send())

        def finish(o, i=i):
            for k in range(len(partners)):
                fcopy(i, o, k).wait_send()
                if relay:
                    rcopy(i, o, k).wait_send()
                    rcopy(i, o, k, True).wait_recv()

        loop(S, finish)


def return_kernel(
    S, T, part_ref, routes_ref, grad_ref, edge_ref, own_ref, full_ref, halo_ref,
    landed, summed, back, fsend, frecv, zsend, zrecv, asend, arecv, hsend, hrecv,
):
    s, p = lax.axis_index("sp"), lax.axis_index("tp")
    cap, d = summed.shape[1], summed.shape[2]
    wait_entry = enter((("sp", S), ("tp", T)))
    wait_entry()

    def cols(q):
        return pl.ds(pl.multiple_of(q * d, d), d)

    def block(t):
        return lax.rem(s + t + 1, S)

    def fcopy(t, r):
        q = lax.rem(p + r, T)
        return remote(
            part_ref.at[block(t), :, cols(q)],
            landed.at[r - 1, block(t)],
            fsend.at[t, r - 1],
            frecv.at[t, r - 1],
            tp=q,
        )

    def zcopy(t, arriving=False):
        row = lax.rem(s - t - 1 + S, S) if arriving else s
        return remote(
            summed.at[block(t)], back.at[row], zsend.at[t], zrecv.at[t], sp=block(t)
        )

    def hcopy(k):
        to = lax.rem(s + (1 if k == 0 else S - 1), S)
        return remote(
            edge_ref.at[1 - k], halo_ref.at[k], hsend.at[k], hrecv.at[k], sp=to
        )

    def start(t):
        for r in range(1, T):
            fcopy(t, r).start()

    loop(S, start)
    for k in range(2):
        hcopy(k).start()

    def total(t):
        for r in range(1, T):
            fcopy(t, r).wait_recv()
        value = part_ref[block(t), :, cols(p)].astype(F32)
        for r in range(1, T):
            value = value + landed[r - 1, block(t)].astype(F32)
        return value.astype(BF16)

    def step(t):
        summed[block(t)] = total(t)

        @pl.when(t > 0)
        def _():
            zcopy(t - 1).start()

    loop(S - 1, step)
    back[s] = total(S - 1)
    zcopy(S - 2).start()

    routes = routes_ref[...]
    first, second = members(routes, S)
    member = (first + second).astype(BF16)
    tri, _ = triangle(routes.shape[0], 1)
    rank = jnp.dot(tri, member, preferred_element_type=F32)
    code = jnp.where(first + second > 0.5, rank, -1.0).astype(jnp.int32)
    slots = lax.broadcasted_iota(jnp.int32, (routes.shape[0], cap), 1)
    loop(S - 1, lambda t: zcopy(t, True).wait_recv())
    value = jnp.zeros((routes.shape[0], d), F32)
    for e in range(S):
        pick = (slots == code[:, e : e + 1]).astype(F32).astype(BF16)
        value = value + jnp.dot(pick, back[e], preferred_element_type=F32)
    value = (grad_ref[...].astype(F32) + value).astype(BF16)
    own_ref[...] = value
    full_ref[:, cols(p)] = value
    loop(S - 1, lambda t: zcopy(t).wait_send())

    def acopy(r, arriving=False):
        at = lax.rem(p - r + T, T) if arriving else p
        return remote(
            own_ref, full_ref.at[:, cols(at)], asend.at[r - 1], arecv.at[r - 1],
            tp=lax.rem(p + r, T),
        )

    for r in range(1, T):
        acopy(r).start()

    def finish(t):
        for r in range(1, T):
            fcopy(t, r).wait_send()

    loop(S, finish)
    for k in range(2):
        hcopy(k).wait()
    for r in range(1, T):
        acopy(r).wait_send()
        acopy(r, True).wait_recv()


def reduce_kernel(
    S, proj_ref, edge_ref, sum_ref, halo_ref, landed, psend, precv, hsend, hrecv
):
    s = lax.axis_index("sp")
    enter((("sp", S),))()

    def hcopy(k):
        to = lax.rem(s + (1 if k == 0 else S - 1), S)
        return remote(
            edge_ref.at[1 - k], halo_ref.at[k], hsend.at[k], hrecv.at[k], sp=to
        )

    def pcopy(o):
        to = lax.rem(s + o + 1, S)
        return remote(proj_ref.at[to], landed.at[o], psend.at[o], precv.at[o], sp=to)

    for k in range(2):
        hcopy(k).start()
    loop(S - 1, lambda o: pcopy(o).start())
    sum_ref[...] = proj_ref[s].astype(F32)

    def step(o):
        pcopy(o).wait_recv()
        sum_ref[...] += landed[o].astype(F32)

    loop(S - 1, step)
    loop(S - 1, lambda o: pcopy(o).wait_send())
    for k in range(2):
        hcopy(k).wait()


def vmem(count):
    return [pl.BlockSpec(memory_space=pltpu.VMEM)] * count


def params(number):
    return pltpu.CompilerParams(collective_id=number, has_side_effects=True)


def rimmed(value, halo):
    s, size = lax.axis_index("sp"), lax.axis_size("sp")
    before = jnp.where(s > 0, halo[0, -1:], 0.0)
    after = jnp.where(s < size - 1, halo[1, :1], 0.0)
    return jnp.concatenate([before, value, after], axis=0)


def edges(value):
    return jnp.stack([value[:8], value[-8:]])


def body(
    routes, route_weights, expert_inputs, out_grad, w_gate, w_up, w_down,
    conv_u, conv_b, conv_c, conv_taps, out_proj,
):
    S, T = lax.axis_size("sp"), lax.axis_size("tp")
    tokens, d = expert_inputs.shape
    channels = conv_u.shape[1]
    cap = 3 * tokens // S
    dma = pltpu.SemaphoreType.DMA
    sent = jax.ShapeDtypeStruct((S, cap, T * d), BF16)
    ways = 2 if T == 4 else T - 1
    relays = (2, S, 2) if T == 4 else (1, 1, 1)
    rows, grads = pl.pallas_call(
        functools.partial(dispatch_kernel, S, T),
        out_shape=(sent, sent),
        in_specs=vmem(4),
        out_specs=tuple(vmem(2)),
        scratch_shapes=[
            pltpu.VMEM((S, cap, d), BF16),
            pltpu.VMEM((S, cap, d), BF16),
            dma((2, S)),
            dma((2, S)),
            dma((2, S, ways)),
            dma((2, S, ways)),
            dma(relays),
            dma(relays),
            dma((2,)),
        ],
        compiler_params=params(0),
        name="dispatch",
    )(routes, route_weights, expert_inputs, out_grad)
    rows = rows.reshape(S * cap, T * d)
    grads = grads.reshape(S * cap, T * d)

    gate_weight, up_weight, down_weight = w_gate[0], w_up[0], w_down[0]
    gate_pre = contract_last(rows, gate_weight)
    up_pre = contract_last(rows, up_weight)
    sigma = jax.nn.sigmoid(gate_pre)
    gate_act = gate_pre * sigma
    hidden = (gate_act * up_pre).astype(BF16)
    grad_hidden = contract_last(grads, down_weight)
    gate_back = (
        grad_hidden * up_pre * sigma * (1.0 + gate_pre * (1.0 - sigma))
    ).astype(BF16)
    up_back = (grad_hidden * gate_act).astype(BF16)
    grad_down = contract_first(hidden, grads).astype(BF16)
    grad_gate = contract_first(gate_back, rows).astype(BF16)
    grad_up = contract_first(up_back, rows).astype(BF16)
    partial_value = jnp.dot(gate_back, gate_weight, preferred_element_type=F32) + jnp.dot(
        up_back, up_weight, preferred_element_type=F32
    )
    partial_value = partial_value.astype(BF16).reshape(S, cap, T * d)

    mixed_in = conv_c.astype(F32) * conv_u.astype(F32)
    halo_shape = jax.ShapeDtypeStruct((2, 8, channels), F32)
    grad_input, grad_full, halo = pl.pallas_call(
        functools.partial(return_kernel, S, T),
        out_shape=(
            jax.ShapeDtypeStruct((tokens, d), BF16),
            jax.ShapeDtypeStruct((tokens, T * d), BF16),
            halo_shape,
        ),
        in_specs=vmem(4),
        out_specs=tuple(vmem(3)),
        scratch_shapes=[
            pltpu.VMEM((T - 1, S, cap, d), BF16),
            pltpu.VMEM((S, cap, d), BF16),
            pltpu.VMEM((S, cap, d), BF16),
            dma((S, T - 1)),
            dma((S, T - 1)),
            dma((S,)),
            dma((S,)),
            dma((T - 1,)),
            dma((T - 1,)),
            dma((2,)),
            dma((2,)),
        ],
        compiler_params=params(1),
        name="bring_back",
    )(partial_value, routes, out_grad, edges(mixed_in))

    padded = rimmed(mixed_in, halo)
    convolved = (
        conv_taps[0] * padded[0:tokens]
        + conv_taps[1] * padded[1 : tokens + 1]
        + conv_taps[2] * padded[2 : tokens + 2]
    )
    conv_out = (conv_b.astype(F32) * convolved).astype(BF16)
    grad_conv = contract_last(grad_full, out_proj)
    grad_b = (grad_conv * convolved).astype(BF16)
    grad_mixed = grad_conv * conv_b.astype(F32)
    proj = contract_first(grad_full, conv_out).astype(BF16)
    width = proj.shape[0] // S
    proj_sum, halo = pl.pallas_call(
        functools.partial(reduce_kernel, S),
        out_shape=(jax.ShapeDtypeStruct((width, channels), F32), halo_shape),
        in_specs=vmem(2),
        out_specs=tuple(vmem(2)),
        scratch_shapes=[
            pltpu.VMEM((S - 1, width, channels), BF16),
            dma((S - 1,)),
            dma((S - 1,)),
            dma((2,)),
            dma((2,)),
        ],
        compiler_params=params(2),
        name="sum_proj",
    )(proj.reshape(S, width, channels), edges(grad_mixed))
    rim = rimmed(grad_mixed, halo)
    grad_z = (
        conv_taps[0] * rim[2 : tokens + 2]
        + conv_taps[1] * rim[1 : tokens + 1]
        + conv_taps[2] * rim[0:tokens]
    )
    grad_c = (grad_z * conv_u.astype(F32)).astype(BF16)
    grad_u = (grad_z * conv_c.astype(F32)).astype(BF16)
    return (
        grad_gate[None], grad_up[None], grad_down[None], grad_input, proj_sum,
        grad_u, grad_b, grad_c,
    )


def solution(mesh):
    in_specs = (
        P("sp", None),
        P("sp", None),
        P("sp", "tp"),
        P("sp", "tp"),
        P("sp", "tp", None),
        P("sp", "tp", None),
        P("sp", "tp", None),
        P("sp", "tp"),
        P("sp", "tp"),
        P("sp", "tp"),
        P(None, "tp"),
        P("tp", None),
    )
    out_specs = (
        P("sp", "tp", None),
        P("sp", "tp", None),
        P("sp", "tp", None),
        P("sp", "tp"),
        P("sp", "tp"),
        P("sp", "tp"),
        P("sp", "tp"),
        P("sp", "tp"),
    )
    return jax.shard_map(body, mesh=mesh, in_specs=in_specs, out_specs=out_specs, check_vma=False)
```

time: 278 us -> 162 us (0.58)
  waiting for transfers between devices: 125 us -> 0 us
  Pallas kernels: 0 us -> 117 us
  blocking collectives: 54.4 us -> 0 us
  local copies, waits for them, and re-layouts: 26.8 us -> 8.19 us
  between operations: 14.1 us -> 0.82 us
  starting transfers between devices: 13.2 us -> 0 us
  matrix products: 35.7 us -> 30.7 us
  other arithmetic: 8.24 us -> 4.34 us
    pallas_call x0 -> x3, Pallas kernels: none -> 117 us  [the longest x1 54.1 us: body(): pl.pallas_call(functools.partial(dispatch_kernel, S, T), out_shape=(sent,...]
    reduce_scatter x2 -> x0, waiting for transfers between devices: 59.2 us -> none  [the longest x1 37.5 us: body(): lax.psum_scatter(partial_value.astype(bf16), 'tp', scatter_dimension=1, t...]
    all_gather x2 -> x0, waiting for transfers between devices: 46.8 us -> none  [the longest x1 30.7 us: body(): lax.all_gather(part_grads, 'tp', axis=1, tiled=True)]
    all_to_all x2 -> x0, blocking collectives: 42.8 us -> none  [the longest x1 23 us: body(): lax.all_to_all(send_rows, 'sp', split_axis=0, concat_axis=0, tiled=True)]
    all_to_all x1 -> x0, waiting for transfers between devices: 16.7 us -> none  [body(): lax.all_to_all(summed, 'sp', split_axis=0, concat_axis=0, tiled=True)]
    all_gather x1 -> x0, blocking collectives: 11.6 us -> none  [body(): grad_full = lax.all_gather(grad_input, 'tp', axis=1, tiled=True)]
    gather x3 -> x0, local copies, waits for them, and re-layouts: 10.2 us -> none  [the longest x1 4.34 us: body(): send_grads = jnp.where(filled, scaled[picked], jnp.zeros((), bf16))]
    ppermute x4 -> x0, starting transfers between devices: 8.3 us -> none  [the longest x2 5.73 us: extended(): before = lax.ppermute(last, axis, up)]
  transfers between devices with their start and end apart: 9 -> 0, of which waited for: 6 -> 0; matrix products, arithmetic and copies ran while one was open for 8% -> 0% of each run, Pallas kernels for 0% -> 0%
where the time goes in v1:
time: 162 us; the launch traced here: 161 us
  Pallas kernels  117 us (72%)
  matrix products  30.7 us (19%)
  local copies, waits for them, and re-layouts  8.19 us (5%)
  other arithmetic  4.34 us (3%)
    pallas_call x1, Pallas kernels, body(): pl.pallas_call(functools.partial(dispatch_kernel, S, T), out_shape=(sent,...  54.1 us
    pallas_call x1, Pallas kernels, body(): pl.pallas_call(functools.partial(return_kernel, S, T), out_shape=(jax.Sha...  48.8 us
    dot_general x4, matrix products, contract_first(): lax.dot_general(left, right, (((0,), (0,)), ((), ())), preferred_element_...  14.8 us
    pallas_call x1, Pallas kernels, body(): pl.pallas_call(functools.partial(reduce_kernel, S), out_shape=(jax.ShapeD...  13.7 us
    dot_general x4, matrix products, contract_last(): lax.dot_general(left, right, (((1,), (1,)), ((), ())), preferred_element_...  10.5 us
    unnamed x30, local copies, waits for them, and re-layouts  7.39 us
    dot_general x1, matrix products, body(): jnp.dot(up_back, up_weight, preferred_element_type=F32)  3.44 us

profile of v1, /device:TPU:0, one launch (start us, length us, event | category | flops | bytes accessed | tf_op | source)
XLA Modules:
  0.0 160.7 jit_solution(2162336482391385879)
XLA Ops:
  0.6 0.0 copy-start
  0.6 1.6 copy.20.routes_ref
  2.2 1.4 copy.21.wts_ref
  3.7 54.1 %dispatch.1 = (bf16[8,72,2048]{2,1,0:T(8,128)(2,1)}, bf16[8,72,2048]{2,1,0:T(8,128)(2,1)}) custom-call(s32[192,2]{1,0:T(8,128)} %copy.20.routes_ref, f32[192,2]{1,0:T(8,128)} %copy.21.wts_ref, bf16[192,512]{1,0:T(8,128)(2,1)} %xin_ref.1, bf16[192,512]{1,0:T(8,128)(2,1)} %grad_ref.1), custom_call_target="tpu_custom_call" | custom-call | tf_op jit(solution)/shard_map/dispatch/pallas_call | solution.py:350
  57.8 0.0 copy-done
  57.8 0.0 copy-start.10
  57.9 0.0 copy-start.12
  57.9 3.8 %fusion.5 = f32[576,704]{1,0:T(8,128)S(1)} fusion(bf16[576,2048]{1,0:T(8,128)(2,1)} %bitcast.64, bf16[1,704,2048]{2,1,0:T(8,128)(2,1)S(1)} %copy-done), kind=kOutput, calls=%fused_computation.9 | convolution fusion | flops 1660944384 | bytes 6864896 | tf_op jit(solution)/shard_map/dot_general | solution.py:22
  61.7 0.0 copy-done.10
  61.7 0.0 copy-done.12
  61.7 0.0 copy-start.9
  61.7 0.0 copy-start.11
  61.8 2.0 %fusion.8 = f32[576,704]{1,0:T(8,128)S(1)} fusion(bf16[576,2048]{1,0:T(8,128)(2,1)S(1)} %bitcast.65, bf16[1,704,2048]{2,1,0:T(8,128)(2,1)S(1)} %copy-done.10), kind=kOutput, calls=%fused_computation.12 | convolution fusion | flops 1660944384 | bytes 6864896 | tf_op jit(solution)/shard_map/dot_general | solution.py:22
  63.8 0.0 copy-done.9
  63.8 0.5 copy-done.11
  64.3 2.5 %multiply_convert_fusion.1 = (bf16[576,704]{1,0:T(8,128)(2,1)S(1)}, bf16[576,704]{1,0:T(8,128)(2,1)S(1)}) fusion(f32[576,704]{1,0:T(8,128)S(1)} %fusion.5, f32[576,704]{1,0:T(8,128)S(1)} %fusion.8, bf16[576,2048]{1,0:T(8,128)(2,1)S(1)} %bitcast.62, bf16[1,704,2048]{2,1,0:T(8,128)(2,1)S(1)} %copy-done.9), kind=kOutput, calls=%fused_computation.18 | convolution fusion | flops 1666215936 | bytes 10108928 | tf_op jit(solution)/shard_map/dot_general | solution.py:22
  66.8 4.0 %fusion = bf16[1,704,2048]{2,1,0:T(8,128)(2,1)} fusion(bf16[576,704]{1,0:T(8,128)(2,1)S(1)} %get-tuple-element.23, bf16[576,2048]{1,0:T(8,128)(2,1)S(1)} %bitcast.66), kind=kOutput, calls=%fused_computation.4 | convolution fusion | flops 1662386176 | bytes 6053888 | tf_op jit(solution)/shard_map/dot_general | solution.py:16
  70.8 4.0 %fusion.1 = bf16[1,704,2048]{2,1,0:T(8,128)(2,1)} fusion(bf16[576,704]{1,0:T(8,128)(2,1)S(1)} %get-tuple-element.22, bf16[576,2048]{1,0:T(8,128)(2,1)S(1)} %bitcast.67), kind=kOutput, calls=%fused_computation.5 | convolution fusion | flops 1662386176 | bytes 6053888 | tf_op jit(solution)/shard_map/dot_general | solution.py:16
  74.8 4.3 %fusion.2 = bf16[1,704,2048]{2,1,0:T(8,128)(2,1)} fusion(bf16[576,2048]{1,0:T(8,128)(2,1)S(1)} %bitcast.63, f32[576,704]{1,0:T(8,128)S(1)} %fusion.8, f32[576,704]{1,0:T(8,128)S(1)} %fusion.5), kind=kOutput, calls=%fused_computation.6 | convolution fusion | flops 1664819200 | bytes 8486912 | tf_op jit(solution)/shard_map/dot_general | solution.py:16
  79.1 2.0 %fusion.3 = f32[576,2048]{1,0:T(8,128)S(1)} fusion(bf16[576,704]{1,0:T(8,128)(2,1)S(1)} %get-tuple-element.23, bf16[1,704,2048]{2,1,0:T(8,128)(2,1)S(1)} %copy-done), kind=kOutput, calls=%fused_computation.7 | convolution fusion | flops 1660944384 | bytes 8413184 | tf_op jit(solution)/shard_map/dot_general | solution.py:386
  81.1 0.0 copy-start.4
  81.1 0.0 copy-start.5
  81.1 3.4 %add_convert_fusion = bf16[576,2048]{1,0:T(8,128)(2,1)} fusion(f32[576,2048]{1,0:T(8,128)S(1)} %fusion.3, bf16[576,704]{1,0:T(8,128)(2,1)S(1)} %get-tuple-element.22, bf16[1,704,2048]{2,1,0:T(8,128)(2,1)S(1)} %copy-done.10), kind=kOutput, calls=%fused_computation | convolution fusion | flops 1663303680 | bytes 10772480 | tf_op jit(solution)/shard_map/dot_general | solution.py:386
  84.5 0.0 copy-start.3
  84.6 0.0 copy-start.1
  84.6 0.0 copy-done.4
  84.6 0.0 copy-done.5
  84.6 0.6 pad_maximum_fusion.4.edge_ref
  85.2 48.8 %bring_back.1 = (bf16[192,512]{1,0:T(8,128)(2,1)}, bf16[192,2048]{1,0:T(8,128)(2,1)}, f32[2,8,128]{2,1,0:T(8,128)}) custom-call(bf16[8,72,2048]{2,1,0:T(8,128)(2,1)} %bitcast.60, s32[192,2]{1,0:T(8,128)} %copy.20.routes_ref, bf16[192,512]{1,0:T(8,128)(2,1)} %grad_ref.1, f32[2,8,128]{2,1,0:T(8,128)} %pad_maximum_fusion.4.edge_ref), custom_call_target="tpu_custom_call" | custom-call | tf_op jit(solution)/shard_map/bring_back/pallas_call | solution.py:393
  134.0 0.7 fusion.27
  134.7 0.8 slice_bitcast_fusion.6
  135.5 0.0 copy-start.6
  135.5 0.0 copy-start.7
  135.5 0.0 copy-start.8
  135.5 0.0 copy-done.3
  135.5 2.4 %convolution_convert_fusion.3 = bf16[2048,128]{1,0:T(8,128)(2,1)} fusion(bf16[192,2048]{1,0:T(8,128)(2,1)} %get-tuple-element.18, bf16[192,128]{1,0:T(8,128)(2,1)S(1)} %copy-done.3, f32[1,128]{1,0:T(1,128)S(1)} %get-tuple-element.35, f32[192,128]{1,0:T(8,128)S(1)} %convert_multiply_fusion.3, f32[1,128]{1,0:T(1,128)S(1)} %get-tuple-element.34, ...), kind=kOutput, calls=%fused_computation.16 | convolution fusion | flops 101171200 | bytes 1460736 | tf_op jit(solution)/shard_map/dot_general | solution.py:16
  138.0 0.0 copy-done.1
  138.0 2.1 %multiply_convert_fusion.4 = (bf16[192,128]{1,0:T(8,128)(2,1)}, f32[192,128]{1,0:T(8,128)S(1)}) fusion(f32[1,128]{1,0:T(1,128)S(1)} %get-tuple-element.35, f32[192,128]{1,0:T(8,128)S(1)} %convert_multiply_fusion.3, f32[128]{0:T(128)S(1)} %get-tuple-element.37, f32[128]{0:T(128)S(1)} %get-tuple-element.38, f32[1,128]{1,0:T(1,128)S(1)} %get-tuple-element.34, ...), kind=kOutput, calls=%fused_computation.42 | convolution fusion | flops 100933632 | bytes 1608192 | tf_op jit(solution)/shard_map/dot_general | solution.py:22
  140.1 0.6 copy-done.2
  140.8 0.0 copy-done.6
  140.8 0.0 copy-done.7
  140.8 0.0 copy-done.8
  140.8 0.6 pad_maximum_fusion.5.edge_ref
  141.4 13.7 %sum_proj.1 = (f32[256,128]{1,0:T(8,128)}, f32[2,8,128]{2,1,0:T(8,128)}) custom-call(bf16[8,256,128]{2,1,0:T(8,128)(2,1)} %bitcast.61, f32[2,8,128]{2,1,0:T(8,128)} %pad_maximum_fusion.5.edge_ref), custom_call_target="tpu_custom_call" | custom-call | tf_op jit(solution)/shard_map/sum_proj/pallas_call | solution.py:431
  155.0 0.7 fusion.30
  155.7 1.7 %fusion.15 = (bf16[192,128]{1,0:T(8,128)(2,1)}, bf16[192,128]{1,0:T(8,128)(2,1)}) fusion(bf16[192,128]{1,0:T(8,128)(2,1)} %param.19, f32[192,128]{1,0:T(8,128)} %copy-done.2, f32[1,128]{1,0:T(1,128)S(1)} %get-tuple-element.33, f32[128]{0:T(128)} %copy-done.7, f32[128]{0:T(128)} %copy-done.8, f32[1,128]{1,0:T(1,128)S(1)} %get-tuple-element.32, ...), kind=kLoop, calls=%fused_computation.28 | loop fusion | flops 319488 | bytes 297472 | tf_op jit(solution)/shard_map/convert_element_type | solution.py:452
  157.5 1.6 %copy.25 = bf16[192,512]{1,0:T(8,128)(2,1)} copy(bf16[192,512]{1,0:T(8,128)(2,1)} %get-tuple-element.50) | data formatting | bytes 393216
  159.1 1.6 copy.26
  (4 shorter events, 0.0 us)
Async XLA Ops:
  0.6 57.2 %copy-start = (bf16[1,704,2048]{2,1,0:T(8,128)(2,1)S(1)}, bf16[1,704,2048]{2,1,0:T(8,128)(2,1)}, u32[]{:S(2)}) copy-start(bf16[1,704,2048]{2,1,0:T(8,128)(2,1)} %param.16) | copy-start | bytes 8650756
  57.8 3.9 %copy-start.10 = (bf16[1,704,2048]{2,1,0:T(8,128)(2,1)S(1)}, bf16[1,704,2048]{2,1,0:T(8,128)(2,1)}, u32[]{:S(2)}) copy-start(bf16[1,704,2048]{2,1,0:T(8,128)(2,1)} %param.17) | copy-start | bytes 8650756
  57.9 3.9 %copy-start.12 = (bf16[8,72,2048]{2,1,0:T(8,128)(2,1)S(1)}, bf16[8,72,2048]{2,1,0:T(8,128)(2,1)}, u32[]{:S(2)}) copy-start(bf16[8,72,2048]{2,1,0:T(8,128)(2,1)} %get-tuple-element.16) | copy-start | bytes 7077892
  61.7 2.1 %copy-start.9 = (bf16[1,704,2048]{2,1,0:T(8,128)(2,1)S(1)}, bf16[1,704,2048]{2,1,0:T(8,128)(2,1)}, u32[]{:S(2)}) copy-start(bf16[1,704,2048]{2,1,0:T(8,128)(2,1)} %param.18) | copy-start | bytes 8650756
  61.7 2.5 %copy-start.11 = (bf16[8,72,2048]{2,1,0:T(8,128)(2,1)S(1)}, bf16[8,72,2048]{2,1,0:T(8,128)(2,1)}, u32[]{:S(2)}) copy-start(bf16[8,72,2048]{2,1,0:T(8,128)(2,1)} %get-tuple-element.15) | copy-start | bytes 7077892
  81.1 3.5 %copy-start.4 = (bf16[192,128]{1,0:T(8,128)(2,1)S(1)}, bf16[192,128]{1,0:T(8,128)(2,1)}, u32[]{:S(2)}) copy-start(bf16[192,128]{1,0:T(8,128)(2,1)} %param.19) | copy-start | bytes 147460
  81.1 3.5 %copy-start.5 = (bf16[192,128]{1,0:T(8,128)(2,1)S(1)}, bf16[192,128]{1,0:T(8,128)(2,1)}, u32[]{:S(2)}) copy-start(bf16[192,128]{1,0:T(8,128)(2,1)} %param.21) | copy-start | bytes 147460
  84.5 51.0 %copy-start.3 = (bf16[192,128]{1,0:T(8,128)(2,1)S(1)}, bf16[192,128]{1,0:T(8,128)(2,1)}, u32[]{:S(2)}) copy-start(bf16[192,128]{1,0:T(8,128)(2,1)} %param.20) | copy-start | bytes 147460
  84.6 53.4 %copy-start.1 = (bf16[128,2048]{1,0:T(8,128)(2,1)S(1)}, bf16[128,2048]{1,0:T(8,128)(2,1)}, u32[]{:S(2)}) copy-start(bf16[128,2048]{1,0:T(8,128)(2,1)} %param.23) | copy-start | bytes 1572868
  135.5 5.2 %copy-start.6 = (f32[128]{0:T(128)}, f32[128]{0:T(128)S(1)}, u32[]{:S(2)}) copy-start(f32[128]{0:T(128)S(1)} %get-tuple-element.36) | copy-start | bytes 1540
  135.5 5.2 %copy-start.7 = (f32[128]{0:T(128)}, f32[128]{0:T(128)S(1)}, u32[]{:S(2)}) copy-start(f32[128]{0:T(128)S(1)} %get-tuple-element.37) | copy-start | bytes 1540
  135.5 5.2 %copy-start.8 = (f32[128]{0:T(128)}, f32[128]{0:T(128)S(1)}, u32[]{:S(2)}) copy-start(f32[128]{0:T(128)S(1)} %get-tuple-element.38) | copy-start | bytes 1540
  140.1 0.6 copy-start.2

commit v2 on v1

--- a/solution.py
+++ b/solution.py
@@ -56,18 +56,17 @@
     )
 
 
-def members(routes, experts):
-    count = routes.shape[0]
-    columns = lax.broadcasted_iota(jnp.int32, (count, experts), 1)
-    first = (routes[:, 0:1] == columns).astype(F32)
-    second = (routes[:, 1:2] == columns).astype(F32)
-    return first, second
-
-
-def triangle(count, earlier_dim):
-    a = lax.broadcasted_iota(jnp.int32, (count, count), earlier_dim)
-    b = lax.broadcasted_iota(jnp.int32, (count, count), 1 - earlier_dim)
-    return (a < b).astype(F32).astype(BF16), (a == b).astype(F32).astype(BF16)
+def slot_codes(routes, experts):
+    count = routes.shape[1]
+    names = lax.broadcasted_iota(jnp.int32, (experts, count), 0)
+    first = (routes[0:1, :] == names).astype(F32)
+    second = (routes[1:2, :] == names).astype(F32)
+    early = lax.broadcasted_iota(jnp.int32, (count, count), 0)
+    late = lax.broadcasted_iota(jnp.int32, (count, count), 1)
+    before = (early < late).astype(F32).astype(BF16)
+    rank = jnp.dot((first + second).astype(BF16), before, preferred_element_type=F32)
+    code = jnp.where(first + second > 0.5, rank, -1.0).astype(jnp.int32)
+    return code, first, second
 
 
 def dispatch_kernel(
@@ -78,22 +77,17 @@
     cap, d = xs.shape[1], xs.shape[2]
     wait_entry = enter((("sp", S), ("tp", T)))
 
-    routes = routes_ref[...]
-    first, second = members(routes, S)
-    weight = first * wts_ref[:, 0:1] + second * wts_ref[:, 1:2]
-    member = (first + second).astype(BF16)
-    tri, eye = triangle(routes.shape[0], 0)
-    rank = contract_first(member, tri)
-    named = contract_first(member, eye)
-    code = jnp.where(named > 0.5, rank, -1.0).astype(jnp.int32)
-    slots = lax.broadcasted_iota(jnp.int32, (cap, routes.shape[0]), 0)
+    code, first, second = slot_codes(routes_ref[...], S)
+    weight = first * wts_ref[0:1, :] + second * wts_ref[1:2, :]
+    slots = lax.broadcasted_iota(jnp.int32, (cap, code.shape[1]), 0)
     xin = xin_ref[...]
-    gin = gin_ref[...].astype(F32)
+    gin = gin_ref[...]
     for e in range(S):
-        pick = (slots == code[e : e + 1, :]).astype(F32).astype(BF16)
+        mask = slots == code[e : e + 1, :]
+        pick = mask.astype(F32).astype(BF16)
         xs[e] = jnp.dot(pick, xin, preferred_element_type=F32).astype(BF16)
-        scaled = (weight[:, e : e + 1] * gin).astype(BF16)
-        gs[e] = jnp.dot(pick, scaled, preferred_element_type=F32).astype(BF16)
+        held = jnp.sum(jnp.where(mask, weight[e : e + 1, :], 0.0), axis=1, keepdims=True)
+        gs[e] = (held * jnp.dot(pick, gin, preferred_element_type=F32)).astype(BF16)
     wait_entry()
 
     arrays = ((xs, x_ref), (gs, g_ref))
@@ -184,29 +178,25 @@
 
 def return_kernel(
     S, T, part_ref, routes_ref, grad_ref, edge_ref, own_ref, full_ref, halo_ref,
-    landed, summed, back, fsend, frecv, zsend, zrecv, asend, arecv, hsend, hrecv,
+    landed, met, passed, summed, back,
+    fsend, frecv, bsend, brecv, zsend, zrecv, asend, arecv, hsend, hrecv,
 ):
     s, p = lax.axis_index("sp"), lax.axis_index("tp")
     cap, d = summed.shape[1], summed.shape[2]
+    relay = T == 4
+    half = d // 2
     wait_entry = enter((("sp", S), ("tp", T)))
     wait_entry()
 
     def cols(q):
         return pl.ds(pl.multiple_of(q * d, d), d)
 
+    def halfcols(q, h):
+        return pl.ds(pl.multiple_of(q * d + h * half, half), half)
+
     def block(t):
         return lax.rem(s + t + 1, S)
 
-    def fcopy(t, r):
-        q = lax.rem(p + r, T)
-        return remote(
-            part_ref.at[block(t), :, cols(q)],
-            landed.at[r - 1, block(t)],
-            fsend.at[t, r - 1],
-            frecv.at[t, r - 1],
-            tp=q,
-        )
-
     def zcopy(t, arriving=False):
         row = lax.rem(s - t - 1 + S, S) if arriving else s
         return remote(
@@ -219,45 +209,114 @@
             edge_ref.at[1 - k], halo_ref.at[k], hsend.at[k], hrecv.at[k], sp=to
         )
 
-    def start(t):
-        for r in range(1, T):
-            fcopy(t, r).start()
-
-    loop(S, start)
+    if relay:
+        xn, yn = p + 1 - 2 * lax.rem(p, 2), lax.rem(p + 2, 4)
+        order = ((xn, yn), (yn, xn))
+
+        def fcopy(t, h, k):
+            to = order[h][0]
+            return remote(
+                part_ref.at[block(t), :, halfcols(3 - p if k else to, h)],
+                landed.at[h, k, block(t)],
+                fsend.at[t, 2 * h + k],
+                frecv.at[t, 2 * h + k],
+                tp=to,
+            )
+
+        def bcopy(t, h):
+            return remote(
+                passed.at[h, block(t)], met.at[h, block(t)],
+                bsend.at[t, h], brecv.at[t, h], tp=order[h][1],
+            )
+
+        def start(t):
+            for k in (1, 0):
+                for h in range(2):
+                    fcopy(t, h, k).start()
+
+        def combine(t):
+            for h in range(2):
+                fcopy(t, h, 1).wait_recv()
+                mine = part_ref[block(t), :, halfcols(order[h][1], h)].astype(F32)
+                passed[h, block(t)] = (mine + landed[h, 1, block(t)].astype(F32)).astype(
+                    BF16
+                )
+
+        def total(t, out, row):
+            for h in range(2):
+                fcopy(t, h, 0).wait_recv()
+                bcopy(t, h).wait_recv()
+                mine = part_ref[block(t), :, halfcols(p, h)].astype(F32)
+                mine = mine + landed[h, 0, block(t)].astype(F32)
+                mine = mine + met[h, block(t)].astype(F32)
+                out[row, :, h * half : (h + 1) * half] = mine.astype(BF16)
+
+        ahead, lag = min(3, S), 2
+    else:
+
+        def fcopy(t, r):
+            q = lax.rem(p + r, T)
+            return remote(
+                part_ref.at[block(t), :, cols(q)],
+                landed.at[r - 1, block(t)],
+                fsend.at[t, r - 1],
+                frecv.at[t, r - 1],
+                tp=q,
+            )
+
+        def start(t):
+            for r in range(1, T):
+                fcopy(t, r).start()
+
+        def total(t, out, row):
+            for r in range(1, T):
+                fcopy(t, r).wait_recv()
+            value = part_ref[block(t), :, cols(p)].astype(F32)
+            for r in range(1, T):
+                value = value + landed[r - 1, block(t)].astype(F32)
+            out[row] = value.astype(BF16)
+
+        ahead, lag = S, 0
+
+    loop(ahead, start)
     for k in range(2):
         hcopy(k).start()
-
-    def total(t):
-        for r in range(1, T):
-            fcopy(t, r).wait_recv()
-        value = part_ref[block(t), :, cols(p)].astype(F32)
-        for r in range(1, T):
-            value = value + landed[r - 1, block(t)].astype(F32)
-        return value.astype(BF16)
+    code, _, _ = slot_codes(routes_ref[...], S)
+    slots = lax.broadcasted_iota(jnp.int32, (cap, code.shape[1]), 0)
 
     def step(t):
-        summed[block(t)] = total(t)
-
-        @pl.when(t > 0)
+        if relay:
+
+            @pl.when(t < S)
+            def _():
+                combine(t)
+
+        @pl.when(jnp.logical_and(t >= lag, t < S - 1 + lag))
         def _():
-            zcopy(t - 1).start()
-
-    loop(S - 1, step)
-    back[s] = total(S - 1)
-    zcopy(S - 2).start()
-
-    routes = routes_ref[...]
-    first, second = members(routes, S)
-    member = (first + second).astype(BF16)
-    tri, _ = triangle(routes.shape[0], 1)
-    rank = jnp.dot(tri, member, preferred_element_type=F32)
-    code = jnp.where(first + second > 0.5, rank, -1.0).astype(jnp.int32)
-    slots = lax.broadcasted_iota(jnp.int32, (routes.shape[0], cap), 1)
+            total(t - lag, summed, block(t - lag))
+
+        if relay:
+
+            @pl.when(t < S)
+            def _():
+                for h in range(2):
+                    bcopy(t, h).start()
+
+            @pl.when(t + ahead < S)
+            def _():
+                start(t + ahead)
+
+        @pl.when(t >= lag + 1)
+        def _():
+            zcopy(t - lag - 1).start()
+
+    loop(S + lag, step)
+    total(S - 1, back, s)
     loop(S - 1, lambda t: zcopy(t, True).wait_recv())
-    value = jnp.zeros((routes.shape[0], d), F32)
+    value = jnp.zeros((code.shape[1], d), F32)
     for e in range(S):
-        pick = (slots == code[:, e : e + 1]).astype(F32).astype(BF16)
-        value = value + jnp.dot(pick, back[e], preferred_element_type=F32)
+        pick = (slots == code[e : e + 1, :]).astype(F32).astype(BF16)
+        value = value + contract_first(pick, back[e])
     value = (grad_ref[...].astype(F32) + value).astype(BF16)
     own_ref[...] = value
     full_ref[:, cols(p)] = value
@@ -274,8 +333,14 @@
         acopy(r).start()
 
     def finish(t):
-        for r in range(1, T):
-            fcopy(t, r).wait_send()
+        if relay:
+            for h in range(2):
+                fcopy(t, h, 0).wait_send()
+                fcopy(t, h, 1).wait_send()
+                bcopy(t, h).wait_send()
+        else:
+            for r in range(1, T):
+                fcopy(t, r).wait_send()
 
     loop(S, finish)
     for k in range(2):
@@ -286,9 +351,12 @@
 
 
 def reduce_kernel(
-    S, proj_ref, edge_ref, sum_ref, halo_ref, landed, psend, precv, hsend, hrecv
+    S, proj_ref, edge_ref, sum_ref, halo_ref,
+    given, pairs, landed, gsend, grecv, psend, precv, hsend, hrecv,
 ):
     s = lax.axis_index("sp")
+    n = S // 2
+    z, c = s // 2, lax.rem(s, 2)
     enter((("sp", S),))()
 
     def hcopy(k):
@@ -297,21 +365,43 @@
             edge_ref.at[1 - k], halo_ref.at[k], hsend.at[k], hrecv.at[k], sp=to
         )
 
+    def at(o):
+        return lax.rem(z + o, n)
+
+    def gcopy(o):
+        return remote(
+            proj_ref.at[2 * at(o) + 1 - c], given.at[at(o)],
+            gsend.at[o], grecv.at[o], sp=s + 1 - 2 * c,
+        )
+
     def pcopy(o):
-        to = lax.rem(s + o + 1, S)
-        return remote(proj_ref.at[to], landed.at[o], psend.at[o], precv.at[o], sp=to)
+        return remote(
+            pairs.at[at(o)], landed.at[o - 1], psend.at[o - 1], precv.at[o - 1],
+            sp=2 * at(o) + c,
+        )
 
     for k in range(2):
         hcopy(k).start()
-    loop(S - 1, lambda o: pcopy(o).start())
-    sum_ref[...] = proj_ref[s].astype(F32)
-
-    def step(o):
+    for o in range(1, n + 1):
+        gcopy(o % n).start()
+
+    def pair(o):
+        gcopy(o).wait_recv()
+        return proj_ref[2 * at(o) + c].astype(F32) + given[at(o)].astype(F32)
+
+    for o in range(1, n):
+        pairs[at(o)] = pair(o).astype(BF16)
+        if o > 1:
+            pcopy(o - 1).start()
+    sum_ref[...] = pair(0)
+    pcopy(n - 1).start()
+    for o in range(1, n):
         pcopy(o).wait_recv()
-        sum_ref[...] += landed[o].astype(F32)
-
-    loop(S - 1, step)
-    loop(S - 1, lambda o: pcopy(o).wait_send())
+        sum_ref[...] += landed[o - 1].astype(F32)
+    for o in range(n):
+        gcopy(o).wait_send()
+        if o > 0:
+            pcopy(o).wait_send()
     for k in range(2):
         hcopy(k).wait()
 
@@ -365,7 +455,7 @@
         ],
         compiler_params=params(0),
         name="dispatch",
-    )(routes, route_weights, expert_inputs, out_grad)
+    )(routes.T, route_weights.T, expert_inputs, out_grad)
     rows = rows.reshape(S * cap, T * d)
     grads = grads.reshape(S * cap, T * d)
 
@@ -388,6 +478,13 @@
     )
     partial_value = partial_value.astype(BF16).reshape(S, cap, T * d)
 
+    if T == 4:
+        pieces = 4
+        shapes = ((2, 2, S, cap, d // 2), (2, S, cap, d // 2), (2, S, cap, d // 2))
+    else:
+        pieces = T - 1
+        shapes = ((T - 1, S, cap, d), (8, 128), (8, 128))
+    landing = [pltpu.VMEM(shape, BF16) for shape in shapes]
     mixed_in = conv_c.astype(F32) * conv_u.astype(F32)
     halo_shape = jax.ShapeDtypeStruct((2, 8, channels), F32)
     grad_input, grad_full, halo = pl.pallas_call(
@@ -400,11 +497,13 @@
         in_specs=vmem(4),
         out_specs=tuple(vmem(3)),
         scratch_shapes=[
-            pltpu.VMEM((T - 1, S, cap, d), BF16),
+            *landing,
             pltpu.VMEM((S, cap, d), BF16),
             pltpu.VMEM((S, cap, d), BF16),
-            dma((S, T - 1)),
-            dma((S, T - 1)),
+            dma((S, pieces)),
+            dma((S, pieces)),
+            dma(relays[1:]),
+            dma(relays[1:]),
             dma((S,)),
             dma((S,)),
             dma((T - 1,)),
@@ -414,7 +513,7 @@
         ],
         compiler_params=params(1),
         name="bring_back",
-    )(partial_value, routes, out_grad, edges(mixed_in))
+    )(partial_value, routes.T, out_grad, edges(mixed_in))
 
     padded = rimmed(mixed_in, halo)
     convolved = (
@@ -434,9 +533,13 @@
         in_specs=vmem(2),
         out_specs=tuple(vmem(2)),
         scratch_shapes=[
-            pltpu.VMEM((S - 1, width, channels), BF16),
-            dma((S - 1,)),
-            dma((S - 1,)),
+            pltpu.VMEM((S // 2, width, channels), BF16),
+            pltpu.VMEM((S // 2, width, channels), BF16),
+            pltpu.VMEM((S // 2 - 1, width, channels), BF16),
+            dma((S // 2,)),
+            dma((S // 2,)),
+            dma((S // 2 - 1,)),
+            dma((S // 2 - 1,)),
             dma((2,)),
             dma((2,)),
         ],

time: 162 us -> 155 us (0.957)
  Pallas kernels: 117 us -> 113 us
  local copies, waits for them, and re-layouts: 8.19 us -> 5.16 us
    pallas_call x1, Pallas kernels: 48.8 us -> 44.9 us  [body(): pl.pallas_call(functools.partial(return_kernel, S, T), out_shape=(jax.Sha...]
    unnamed x30 -> x28, local copies, waits for them, and re-layouts: 7.39 us -> 4.36 us
where the time goes in v2:
time: 155 us; the launch traced here: 154 us
  Pallas kernels  113 us (73%)
  matrix products  30.7 us (20%)
  local copies, waits for them, and re-layouts  5.16 us (3%)
  other arithmetic  4.34 us (3%)
    pallas_call x1, Pallas kernels, body(): pl.pallas_call(functools.partial(dispatch_kernel, S, T), out_shape=(sent,...  54 us
    pallas_call x1, Pallas kernels, body(): pl.pallas_call(functools.partial(return_kernel, S, T), out_shape=(jax.Sha...  44.9 us
    dot_general x4, matrix products, contract_first(): lax.dot_general(left, right, (((0,), (0,)), ((), ())), preferred_element_...  14.8 us
    pallas_call x1, Pallas kernels, body(): pl.pallas_call(functools.partial(reduce_kernel, S), out_shape=(jax.ShapeD...  14.4 us
    dot_general x4, matrix products, contract_last(): lax.dot_general(left, right, (((1,), (1,)), ((), ())), preferred_element_...  10.5 us
    unnamed x28, local copies, waits for them, and re-layouts  4.36 us
    dot_general x1, matrix products, body(): jnp.dot(up_back, up_weight, preferred_element_type=F32)  3.44 us

profile of v2, /device:TPU:0, one launch (start us, length us, event | category | flops | bytes accessed | tf_op | source)
XLA Modules:
  0.0 154.3 jit_solution(17056196496389727305)
XLA Ops:
  0.6 0.0 copy-start
  0.6 54.0 %dispatch.1 = (bf16[8,72,2048]{2,1,0:T(8,128)(2,1)}, bf16[8,72,2048]{2,1,0:T(8,128)(2,1)}) custom-call(s32[2,192]{1,0:T(2,128)} %bitcast.64, f32[2,192]{1,0:T(2,128)} %bitcast.66, bf16[192,512]{1,0:T(8,128)(2,1)} %xin_ref.1, bf16[192,512]{1,0:T(8,128)(2,1)} %grad_ref.1), custom_call_target="tpu_custom_call" | custom-call | tf_op jit(solution)/shard_map/dispatch/pallas_call | solution.py:440
  54.6 0.0 copy-done
  54.6 0.0 copy-start.10
  54.6 0.0 copy-start.12
  54.7 3.9 %fusion.5 = f32[576,704]{1,0:T(8,128)S(1)} fusion(bf16[576,2048]{1,0:T(8,128)(2,1)} %bitcast.69, bf16[1,704,2048]{2,1,0:T(8,128)(2,1)S(1)} %copy-done), kind=kOutput, calls=%fused_computation.9 | convolution fusion | flops 1660944384 | bytes 6864896 | tf_op jit(solution)/shard_map/dot_general | solution.py:22
  58.5 0.0 copy-done.10
  58.5 0.0 copy-done.12
  58.5 0.0 copy-start.9
  58.5 0.0 copy-start.11
  58.6 2.0 %fusion.8 = f32[576,704]{1,0:T(8,128)S(1)} fusion(bf16[576,2048]{1,0:T(8,128)(2,1)S(1)} %bitcast.70, bf16[1,704,2048]{2,1,0:T(8,128)(2,1)S(1)} %copy-done.10), kind=kOutput, calls=%fused_computation.12 | convolution fusion | flops 1660944384 | bytes 6864896 | tf_op jit(solution)/shard_map/dot_general | solution.py:22
  60.6 0.0 copy-done.9
  60.6 0.5 copy-done.11
  61.1 2.5 %multiply_convert_fusion.1 = (bf16[576,704]{1,0:T(8,128)(2,1)S(1)}, bf16[576,704]{1,0:T(8,128)(2,1)S(1)}) fusion(f32[576,704]{1,0:T(8,128)S(1)} %fusion.5, f32[576,704]{1,0:T(8,128)S(1)} %fusion.8, bf16[576,2048]{1,0:T(8,128)(2,1)S(1)} %bitcast.67, bf16[1,704,2048]{2,1,0:T(8,128)(2,1)S(1)} %copy-done.9), kind=kOutput, calls=%fused_computation.18 | convolution fusion | flops 1666215936 | bytes 10108928 | tf_op jit(solution)/shard_map/dot_general | solution.py:22
  63.5 4.0 %fusion = bf16[1,704,2048]{2,1,0:T(8,128)(2,1)} fusion(bf16[576,704]{1,0:T(8,128)(2,1)S(1)} %get-tuple-element.23, bf16[576,2048]{1,0:T(8,128)(2,1)S(1)} %bitcast.71), kind=kOutput, calls=%fused_computation.4 | convolution fusion | flops 1662386176 | bytes 6053888 | tf_op jit(solution)/shard_map/dot_general | solution.py:16
  67.6 4.0 %fusion.1 = bf16[1,704,2048]{2,1,0:T(8,128)(2,1)} fusion(bf16[576,704]{1,0:T(8,128)(2,1)S(1)} %get-tuple-element.22, bf16[576,2048]{1,0:T(8,128)(2,1)S(1)} %bitcast.72), kind=kOutput, calls=%fused_computation.5 | convolution fusion | flops 1662386176 | bytes 6053888 | tf_op jit(solution)/shard_map/dot_general | solution.py:16
  71.6 4.3 %fusion.2 = bf16[1,704,2048]{2,1,0:T(8,128)(2,1)} fusion(bf16[576,2048]{1,0:T(8,128)(2,1)S(1)} %bitcast.68, f32[576,704]{1,0:T(8,128)S(1)} %fusion.8, f32[576,704]{1,0:T(8,128)S(1)} %fusion.5), kind=kOutput, calls=%fused_computation.6 | convolution fusion | flops 1664819200 | bytes 8486912 | tf_op jit(solution)/shard_map/dot_general | solution.py:16
  75.9 2.0 %fusion.3 = f32[576,2048]{1,0:T(8,128)S(1)} fusion(bf16[576,704]{1,0:T(8,128)(2,1)S(1)} %get-tuple-element.23, bf16[1,704,2048]{2,1,0:T(8,128)(2,1)S(1)} %copy-done), kind=kOutput, calls=%fused_computation.7 | convolution fusion | flops 1660944384 | bytes 8413184 | tf_op jit(solution)/shard_map/dot_general | solution.py:476
  77.9 0.0 copy-start.4
  77.9 0.0 copy-start.5
  77.9 3.4 %add_convert_fusion = bf16[576,2048]{1,0:T(8,128)(2,1)} fusion(f32[576,2048]{1,0:T(8,128)S(1)} %fusion.3, bf16[576,704]{1,0:T(8,128)(2,1)S(1)} %get-tuple-element.22, bf16[1,704,2048]{2,1,0:T(8,128)(2,1)S(1)} %copy-done.10), kind=kOutput, calls=%fused_computation | convolution fusion | flops 1663303680 | bytes 10772480 | tf_op jit(solution)/shard_map/dot_general | solution.py:476
  81.3 0.0 copy-start.3
  81.3 0.0 copy-start.1
  81.3 0.0 copy-done.4
  81.3 0.0 copy-done.5
  81.4 0.6 pad_maximum_fusion.4.edge_ref
  82.0 44.9 %bring_back.1 = (bf16[192,512]{1,0:T(8,128)(2,1)}, bf16[192,2048]{1,0:T(8,128)(2,1)}, f32[2,8,128]{2,1,0:T(8,128)}) custom-call(bf16[8,72,2048]{2,1,0:T(8,128)(2,1)} %bitcast.62, s32[2,192]{1,0:T(2,128)} %bitcast.65, bf16[192,512]{1,0:T(8,128)(2,1)} %grad_ref.1, f32[2,8,128]{2,1,0:T(8,128)} %pad_maximum_fusion.4.edge_ref), custom_call_target="tpu_custom_call" | custom-call | tf_op jit(solution)/shard_map/bring_back/pallas_call | solution.py:490
  126.9 0.7 fusion.27
  127.6 0.8 slice_bitcast_fusion.6
  128.4 0.0 copy-start.6
  128.4 0.0 copy-start.7
  128.4 0.0 copy-start.8
  128.4 0.0 copy-done.3
  128.4 2.4 %convolution_convert_fusion.3 = bf16[2048,128]{1,0:T(8,128)(2,1)} fusion(bf16[192,2048]{1,0:T(8,128)(2,1)} %get-tuple-element.18, bf16[192,128]{1,0:T(8,128)(2,1)S(1)} %copy-done.3, f32[1,128]{1,0:T(1,128)S(1)} %get-tuple-element.35, f32[192,128]{1,0:T(8,128)S(1)} %convert_multiply_fusion.3, f32[1,128]{1,0:T(1,128)S(1)} %get-tuple-element.34, ...), kind=kOutput, calls=%fused_computation.16 | convolution fusion | flops 101171200 | bytes 1460736 | tf_op jit(solution)/shard_map/dot_general | solution.py:16
  130.8 0.0 copy-done.1
  130.8 2.1 %multiply_convert_fusion.4 = (bf16[192,128]{1,0:T(8,128)(2,1)}, f32[192,128]{1,0:T(8,128)S(1)}) fusion(f32[1,128]{1,0:T(1,128)S(1)} %get-tuple-element.35, f32[192,128]{1,0:T(8,128)S(1)} %convert_multiply_fusion.3, f32[128]{0:T(128)S(1)} %get-tuple-element.37, f32[128]{0:T(128)S(1)} %get-tuple-element.38, f32[1,128]{1,0:T(1,128)S(1)} %get-tuple-element.34, ...), kind=kOutput, calls=%fused_computation.42 | convolution fusion | flops 100933632 | bytes 1608192 | tf_op jit(solution)/shard_map/dot_general | solution.py:22
  132.9 0.0 copy-start.2
  132.9 0.6 copy-done.2
  133.6 0.0 copy-done.6
  133.6 0.0 copy-done.7
  133.6 0.0 copy-done.8
  133.6 0.6 pad_maximum_fusion.5.edge_ref
  134.2 14.4 %sum_proj.1 = (f32[256,128]{1,0:T(8,128)}, f32[2,8,128]{2,1,0:T(8,128)}) custom-call(bf16[8,256,128]{2,1,0:T(8,128)(2,1)} %bitcast.63, f32[2,8,128]{2,1,0:T(8,128)} %pad_maximum_fusion.5.edge_ref), custom_call_target="tpu_custom_call" | custom-call | tf_op jit(solution)/shard_map/sum_proj/pallas_call | solution.py:530
  148.6 0.7 fusion.30
  149.3 1.7 %fusion.15 = (bf16[192,128]{1,0:T(8,128)(2,1)}, bf16[192,128]{1,0:T(8,128)(2,1)}) fusion(bf16[192,128]{1,0:T(8,128)(2,1)} %param.19, f32[192,128]{1,0:T(8,128)} %copy-done.2, f32[1,128]{1,0:T(1,128)S(1)} %get-tuple-element.33, f32[128]{0:T(128)} %copy-done.7, f32[128]{0:T(128)} %copy-done.8, f32[1,128]{1,0:T(1,128)S(1)} %get-tuple-element.32, ...), kind=kLoop, calls=%fused_computation.28 | loop fusion | flops 319488 | bytes 297472 | tf_op jit(solution)/shard_map/convert_element_type | solution.py:555
  151.1 1.6 %copy.22 = bf16[192,512]{1,0:T(8,128)(2,1)} copy(bf16[192,512]{1,0:T(8,128)(2,1)} %get-tuple-element.50) | data formatting | bytes 393216
  152.7 1.6 %copy.23 = f32[256,128]{1,0:T(8,128)} copy(f32[256,128]{1,0:T(8,128)} %get-tuple-element.51) | data formatting | bytes 262144
  (3 shorter events, 0.0 us)
Async XLA Ops:
  0.6 54.0 %copy-start = (bf16[1,704,2048]{2,1,0:T(8,128)(2,1)S(1)}, bf16[1,704,2048]{2,1,0:T(8,128)(2,1)}, u32[]{:S(2)}) copy-start(bf16[1,704,2048]{2,1,0:T(8,128)(2,1)} %param.16) | copy-start | bytes 8650756
  54.6 3.9 %copy-start.10 = (bf16[1,704,2048]{2,1,0:T(8,128)(2,1)S(1)}, bf16[1,704,2048]{2,1,0:T(8,128)(2,1)}, u32[]{:S(2)}) copy-start(bf16[1,704,2048]{2,1,0:T(8,128)(2,1)} %param.17) | copy-start | bytes 8650756
  54.6 3.9 %copy-start.12 = (bf16[8,72,2048]{2,1,0:T(8,128)(2,1)S(1)}, bf16[8,72,2048]{2,1,0:T(8,128)(2,1)}, u32[]{:S(2)}) copy-start(bf16[8,72,2048]{2,1,0:T(8,128)(2,1)} %get-tuple-element.16) | copy-start | bytes 7077892
  58.5 2.1 %copy-start.9 = (bf16[1,704,2048]{2,1,0:T(8,128)(2,1)S(1)}, bf16[1,704,2048]{2,1,0:T(8,128)(2,1)}, u32[]{:S(2)}) copy-start(bf16[1,704,2048]{2,1,0:T(8,128)(2,1)} %param.18) | copy-start | bytes 8650756
  58.5 2.5 %copy-start.11 = (bf16[8,72,2048]{2,1,0:T(8,128)(2,1)S(1)}, bf16[8,72,2048]{2,1,0:T(8,128)(2,1)}, u32[]{:S(2)}) copy-start(bf16[8,72,2048]{2,1,0:T(8,128)(2,1)} %get-tuple-element.15) | copy-start | bytes 7077892
  77.9 3.5 %copy-start.4 = (bf16[192,128]{1,0:T(8,128)(2,1)S(1)}, bf16[192,128]{1,0:T(8,128)(2,1)}, u32[]{:S(2)}) copy-start(bf16[192,128]{1,0:T(8,128)(2,1)} %param.19) | copy-start | bytes 147460
  77.9 3.5 %copy-start.5 = (bf16[192,128]{1,0:T(8,128)(2,1)S(1)}, bf16[192,128]{1,0:T(8,128)(2,1)}, u32[]{:S(2)}) copy-start(bf16[192,128]{1,0:T(8,128)(2,1)} %param.21) | copy-start | bytes 147460
  81.3 47.0 %copy-start.3 = (bf16[192,128]{1,0:T(8,128)(2,1)S(1)}, bf16[192,128]{1,0:T(8,128)(2,1)}, u32[]{:S(2)}) copy-start(bf16[192,128]{1,0:T(8,128)(2,1)} %param.20) | copy-start | bytes 147460
  81.3 49.5 %copy-start.1 = (bf16[128,2048]{1,0:T(8,128)(2,1)S(1)}, bf16[128,2048]{1,0:T(8,128)(2,1)}, u32[]{:S(2)}) copy-start(bf16[128,2048]{1,0:T(8,128)(2,1)} %param.23) | copy-start | bytes 1572868
  128.4 5.2 %copy-start.6 = (f32[128]{0:T(128)}, f32[128]{0:T(128)S(1)}, u32[]{:S(2)}) copy-start(f32[128]{0:T(128)S(1)} %get-tuple-element.36) | copy-start | bytes 1540
  128.4 5.2 %copy-start.7 = (f32[128]{0:T(128)}, f32[128]{0:T(128)S(1)}, u32[]{:S(2)}) copy-start(f32[128]{0:T(128)S(1)} %get-tuple-element.37) | copy-start | bytes 1540
  128.4 5.2 %copy-start.8 = (f32[128]{0:T(128)}, f32[128]{0:T(128)S(1)}, u32[]{:S(2)}) copy-start(f32[128]{0:T(128)S(1)} %get-tuple-element.38) | copy-start | bytes 1540
  132.9 0.6 copy-start.2
